TPU v7x, 512 devices: a whole 4x4x16 slice. The times are simulated.
512 devices in a mesh: sp: 16 (over z), fs: 4 (over y), tp: 8 (over x, core).
Axes of the slice: x: 4, y: 4, z: 16, core: 2. Of those that a mesh axis runs over, the one named last changes fastest.
Arguments:
- tokens: bfloat16 [4, 16384, 2048], P('fs', ('sp', 'tp')), may hold values from -6 to 6
- input_norm_gain: float32 [2048], replicated, may hold values from 0.1 to 1.9
- earlier_gate: bfloat16 [2048, 1024], P(('sp', 'fs'), 'tp'), may hold values from -0.125 to 0.125
- later_gate: bfloat16 [2048, 1024], P(('sp', 'fs'), 'tp'), may hold values from -0.125 to 0.125
- convolution_input: bfloat16 [2048, 1024], P(('sp', 'fs'), 'tp'), may hold values from -0.125 to 0.125
- convolution_taps: float32 [3, 1024], P(None, 'tp'), may hold values from -3 to 3
- receptance: bfloat16 [2048, 1024], P(('sp', 'fs'), 'tp'), may hold values from -0.125 to 0.125
- key_matrix: bfloat16 [2048, 1024], P(('sp', 'fs'), 'tp'), may hold values from -0.125 to 0.125
- value_matrix: bfloat16 [2048, 1024], P(('sp', 'fs'), 'tp'), may hold values from -0.125 to 0.125
- decay_matrix: bfloat16 [2048, 1024], P(('sp', 'fs'), 'tp'), may hold values from -0.125 to 0.125
- rate_matrix: bfloat16 [2048, 1024], P(('sp', 'fs'), 'tp'), may hold values from -0.125 to 0.125
- decay_floor: float32 [1024], P('tp'), may hold values from -16 to -3.4
- rate_offset: float32 [1024], P('tp'), may hold values from -7.5 to 1
- decay_spike: float32 [4, 16384, 1024], P('fs', 'sp', 'tp'), may hold values from -1.3 to 0
- initial_state: float32 [4, 16, 64, 64], P('fs', 'tp'), may hold values from -768 to 768
- head_norm_gain: float32 [1024], P('tp'), may hold values from 0.1 to 1.9
- convolution_output: bfloat16 [1024, 2048], P('tp', ('sp', 'fs')), may hold values from -0.125 to 0.125
- state_heads_output: bfloat16 [1024, 2048], P('tp', ('sp', 'fs')), may hold values from -0.125 to 0.125
Outputs:
- mixed: bfloat16 [4, 16384, 2048], P('fs', ('sp', 'tp'))
All inputs are finite; a program needn't handle non-finite values.
Results may differ from a plain program's by a relative error of at most 0.02.
Values may be sent and summed in bfloat16 or wider, within the bound.
No kernel may reach another device: no remote copies, remote signals or barrier semaphores. Data moves between devices by JAX's collectives and lax.ppermute only.
A program may use at most 64 MiB of HBM per device.

v0:
```python
import jax
import jax.numpy as jnp
from jax import lax
from jax.sharding import PartitionSpec as P

HEAD_WIDTH = 64
BLOCK = 64
norm_eps = 1e-06
key_eps = 1e-06


def passed_along(block, axis, distance):
    devices = range(lax.axis_size(axis))
    route = [(i - distance, i) for i in devices if i - distance in devices]
    return lax.ppermute(block, axis, route)


def side_by_side(arrays, axis, dim, along):
    widths = [a.shape[along] for a in arrays]
    both = jnp.concatenate(arrays, axis=along)
    out = lax.all_gather(both, axis, axis=dim, tiled=True)
    return tuple(jnp.split(out, [sum(widths[:k]) for k in range(1, len(widths))], axis=along))


def from_everyone(x, axis):
    devices = lax.axis_size(axis)
    return lax.all_to_all(jnp.broadcast_to(x[None], (devices, *x.shape)), axis, 0, 0, tiled=True)


def collected_together(x, axis):
    leaves = jax.tree.leaves(x)
    order = sorted(range(len(leaves)), key=lambda k: -leaves[k].size)
    width = (1, *leaves[order[0]].shape)[-1]
    lines = [
        jnp.pad(leaves[k].reshape(-1), (0, -leaves[k].size % width)).reshape(-1, width)
        for k in order
    ]
    both, at, found = (from_everyone(jnp.concatenate(lines), axis), 0, {})
    for k, line in zip(order, lines):
        piece = both[:, at : at + len(line)].reshape(len(both), -1)
        found[k] = piece[:, : leaves[k].size].reshape(-1, *leaves[k].shape)
        at += len(line)
    numbers = iter(range(len(leaves)))
    return jax.tree.map(lambda _: found[next(numbers)], x)


def combined_pairwise(pieces, combine):
    while len(jax.tree.leaves(pieces)[0]) > 1:
        pieces = jax.vmap(combine)(
            *(jax.tree.map(lambda part: part[side::2], pieces) for side in (0, 1))
        )
    return jax.tree.map(lambda part: part[0], pieces)


def entering(x, axis, combine, identity):
    devices, position = (lax.axis_size(axis), lax.axis_index(axis))
    passed = jnp.arange(devices) < position

    def kept(part, zero, own):
        part = jnp.where(
            passed.reshape(-1, *(1 for _ in own.shape)),
            part.astype(own.dtype),
            jnp.asarray(zero, own.dtype),
        )
        return part

    pieces = collected_together(
        jax.tree.map(lambda part, kind: part.astype(kind), x, (jnp.bfloat16, jnp.bfloat16)), axis
    )
    return combined_pairwise(jax.tree.map(kept, pieces, identity, x), combine)


def gather_turned(arrays, axis, dims):
    turned = [jnp.moveaxis(a, dim, 0) for a, dim in zip(arrays, dims)]
    both = jnp.concatenate([t.reshape(len(t), -1) for t in turned], axis=1)
    out, at, outs = (lax.all_gather(both, axis, axis=0, tiled=True), 0, [])
    for t, dim in zip(turned, dims):
        piece = out[:, at : at + t[0].size].reshape(-1, *t.shape[1:])
        outs.append(jnp.moveaxis(piece, 0, dim))
        at += t[0].size
    return tuple(outs)


def rms_rows(activations, gain_vector):
    values = activations.astype(jnp.float32)
    inv_scale = lax.rsqrt(jnp.mean(values * values, axis=-1, keepdims=True) + norm_eps)
    return (values * inv_scale * gain_vector).astype(jnp.bfloat16)


def project(activations, weight):
    return jnp.dot(activations, weight, preferred_element_type=jnp.float32).astype(jnp.bfloat16)


def conv_branch(pre_values, post_values, conv_values, convolution_taps):
    product = pre_values.astype(jnp.float32) * conv_values.astype(jnp.float32)
    reach_rows = convolution_taps.shape[0] - 1
    sequence_rows = product.shape[0]
    edge_rows = passed_along(product[sequence_rows - reach_rows :], "sp", 1)
    padded = jnp.concatenate([edge_rows, product], axis=0)
    filtered = convolution_taps[0] * padded[0:sequence_rows]
    for offset in range(1, convolution_taps.shape[0]):
        filtered = filtered + convolution_taps[offset] * padded[offset : offset + sequence_rows]
    return (post_values.astype(jnp.float32) * filtered).astype(jnp.bfloat16)


def pairs(left_side, right_side, allowed):
    return jnp.where(allowed, jnp.einsum("thj,shj->hts", left_side, right_side), 0.0)


def block_pass(carried, inputs):
    queries, key_rows, value_rows, unit_keys, beta_rows, logarithm_decay = inputs
    span_rows = logarithm_decay.shape[0]
    cumulative = jnp.cumsum(logarithm_decay, axis=0)
    previous = cumulative - logarithm_decay
    middle = cumulative[span_rows // 2]
    later_index = lax.broadcasted_iota(jnp.int32, (span_rows, span_rows), 0)
    earlier_index = lax.broadcasted_iota(jnp.int32, (span_rows, span_rows), 1)
    strict = (later_index > earlier_index)[None]
    inclusive = (later_index >= earlier_index)[None]
    ask_keys = unit_keys * jnp.exp(previous - middle)
    ask_reads = queries * jnp.exp(cumulative - middle)
    give_keys = key_rows * jnp.exp(middle - cumulative)
    give_betas = beta_rows * jnp.exp(middle - cumulative)
    key_ask = pairs(ask_keys, give_keys, strict)
    beta_ask = pairs(ask_keys, give_betas, strict)
    key_read = pairs(ask_reads, give_keys, inclusive)
    beta_read = pairs(ask_reads, give_betas, inclusive)
    extended = jnp.concatenate([value_rows, jnp.zeros_like(value_rows)], axis=2)
    from_start = jnp.einsum("thj,hrj->htr", unit_keys * jnp.exp(previous), carried)
    right_side = from_start + jnp.einsum("hts,shr->htr", key_ask, extended)
    system = beta_ask + jnp.eye(span_rows, dtype=jnp.float32)[None]
    removed = jax.scipy.linalg.solve_triangular(system, right_side, lower=True, unit_diagonal=True)
    outputs = (
        jnp.einsum("thj,hrj->thr", queries * jnp.exp(cumulative), carried)
        + jnp.einsum("hts,shr->thr", key_read, extended)
        - jnp.einsum("hts,hsr->thr", beta_read, removed)
    )
    closing = cumulative[span_rows - 1]
    tail_decay = jnp.exp(closing - cumulative)
    carried = (
        carried * jnp.exp(closing)[:, None, :]
        + jnp.einsum("shr,shj->hrj", extended, key_rows * tail_decay)
        - jnp.einsum("hsr,shj->hrj", removed, beta_rows * tail_decay)
    )
    return (carried, outputs)


def compose(earlier, later):
    return (
        jnp.einsum("hij,hjk->hik", earlier[0], later[0]),
        jnp.einsum("hij,hjk->hik", earlier[1], later[0]) + later[1],
    )


def on_device(
    tokens,
    input_norm_gain,
    earlier_gate,
    later_gate,
    convolution_input,
    convolution_taps,
    receptance,
    key_matrix,
    value_matrix,
    decay_matrix,
    rate_matrix,
    decay_floor,
    rate_offset,
    decay_spike,
    initial_state,
    head_norm_gain,
    convolution_output,
    state_heads_output,
):
    normed = rms_rows(tokens[0], input_norm_gain)
    channels = earlier_gate.shape[1]
    gathered = side_by_side(
        (
            earlier_gate,
            later_gate,
            convolution_input,
            receptance,
            key_matrix,
            value_matrix,
            decay_matrix,
            rate_matrix,
        ),
        ("sp", "fs"),
        0,
        1,
    )
    piece = lax.all_gather(normed, "tp", axis=0, tiled=True)
    projected = jnp.concatenate([project(piece, weight) for weight in gathered], axis=1)
    pieces = jnp.split(projected, 8, axis=1)
    conv_mixed = conv_branch(pieces[0], pieces[1], pieces[2], convolution_taps)
    queries_raw, keys_raw, values_raw, decay_pre, rate_pre = pieces[3:]
    sequence_rows = queries_raw.shape[0]
    present_heads = channels // HEAD_WIDTH

    def by_heads(array):
        return array.astype(jnp.float32).reshape(sequence_rows, present_heads, HEAD_WIDTH)

    queries = by_heads(queries_raw)
    key_rows = by_heads(keys_raw)
    value_rows = by_heads(values_raw)
    logarithm_decay = -jnp.exp(
        decay_floor.reshape(present_heads, HEAD_WIDTH) + jnp.tanh(by_heads(decay_pre))
    )
    logarithm_decay = logarithm_decay + decay_spike[0].reshape(
        sequence_rows, present_heads, HEAD_WIDTH
    )
    learn_rate = jax.nn.sigmoid(rate_offset.reshape(present_heads, HEAD_WIDTH) + by_heads(rate_pre))
    unit_keys = key_rows * lax.rsqrt(jnp.sum(key_rows * key_rows, axis=-1, keepdims=True) + key_eps)
    beta_rows = learn_rate * unit_keys
    blocks = sequence_rows // BLOCK

    def in_blocks(array):
        return array.reshape(blocks, BLOCK, present_heads, HEAD_WIDTH)

    identity = jnp.broadcast_to(
        jnp.eye(HEAD_WIDTH, dtype=jnp.float32), (present_heads, HEAD_WIDTH, HEAD_WIDTH)
    )
    initial_rows = jnp.concatenate(
        [jnp.zeros((present_heads, HEAD_WIDTH, HEAD_WIDTH), jnp.float32), identity], axis=1
    )
    ending, outputs = lax.scan(
        block_pass,
        initial_rows,
        tuple(
            (
                in_blocks(array)
                for array in (queries, key_rows, value_rows, unit_keys, beta_rows, logarithm_decay)
            )
        ),
    )
    outputs = outputs.reshape(sequence_rows, present_heads, 2 * HEAD_WIDTH)
    carry_source = ending[:, :HEAD_WIDTH, :]
    carry_map = ending[:, HEAD_WIDTH:, :]
    first_state = initial_state[0]
    prefix_map, prefix_source = entering(
        (carry_map, carry_source), "sp", compose, (identity, jnp.zeros_like(carry_source))
    )
    opening_state = jnp.einsum("hvj,hjk->hvk", first_state, prefix_map) + prefix_source
    reads = outputs[..., :HEAD_WIDTH] + jnp.einsum(
        "thj,hvj->thv", outputs[..., HEAD_WIDTH:], opening_state
    )
    centered = reads - jnp.mean(reads, axis=-1, keepdims=True)
    variance = jnp.mean(centered * centered, axis=-1, keepdims=True)
    state_mixed = (
        centered
        * lax.rsqrt(variance + HEAD_WIDTH * 1e-05)
        * head_norm_gain.reshape(present_heads, HEAD_WIDTH)
    )
    state_mixed = state_mixed.reshape(sequence_rows, channels).astype(jnp.bfloat16)
    conv_whole, state_whole = gather_turned(
        (convolution_output, state_heads_output), ("sp", "fs"), (1, 1)
    )
    mixed = lax.psum_scatter(
        (
            jnp.dot(conv_mixed, conv_whole, preferred_element_type=jnp.float32)
            + jnp.dot(state_mixed, state_whole, preferred_element_type=jnp.float32)
        ).astype(jnp.bfloat16),
        "tp",
        scatter_dimension=0,
        tiled=True,
    )
    return mixed[None]


def solution(mesh):
    placed = (
        P("fs", ("sp", "tp"), None),
        P(),
        P(("sp", "fs"), "tp"),
        P(("sp", "fs"), "tp"),
        P(("sp", "fs"), "tp"),
        P(None, "tp"),
        P(("sp", "fs"), "tp"),
        P(("sp", "fs"), "tp"),
        P(("sp", "fs"), "tp"),
        P(("sp", "fs"), "tp"),
        P(("sp", "fs"), "tp"),
        P("tp"),
        P("tp"),
        P("fs", "sp", "tp"),
        P("fs", "tp", None, None),
        P("tp"),
        P("tp", ("sp", "fs")),
        P("tp", ("sp", "fs")),
    )
    return jax.shard_map(
        on_device,
        mesh=mesh,
        in_specs=placed,
        out_specs=P("fs", ("sp", "tp"), None),
        check_vma=False,
    )
```

profile of v0, /device:TPU:8, one launch (start us, length us, event | category | flops | bytes accessed | tf_op | source)
XLA Modules:
  0.0 573.6 jit_solution(10139626129675810700)
XLA Ops:
  6.5 1.3 fusion.63
  7.8 2.0 fusion.65
  16.2 1.3 pad_maximum_fusion.2
  18.3 2.6 reshape_squeeze.3
  21.9 32.2 %all-gather.4.cloned.1.call-done = bf16[1024,2048]{1,0:T(8,128)(2,1)} async-done(((bf16[128,2048]{1,0:T(8,128)(2,1)}), bf16[1024,2048]{1,0:T(8,128)(2,1)}) %all-gather.4.cloned.1.call-update) | async-done | bytes 4194320 | tf_op jit(solution)/shard_map/all_gather | solution.py:192
  54.1 147.6 %all-gather.6.cloned.1.call-done = bf16[2048,1024]{1,0:T(8,128)(2,1)} async-done(((bf16[32,1024]{1,0:T(8,128)(2,1)}), bf16[2048,1024]{1,0:T(8,128)(2,1)}) %all-gather.6.cloned.1.call-update) | async-done | bytes 4194320 | tf_op jit(solution)/shard_map/all_gather | solution.py:21
  201.7 3.8 bitcast_reduce_fusion
  206.5 1.0 copy.76
  207.5 4.3 fusion.51
  211.9 1.6 reshape.141
  213.5 4.4 fusion.55
  217.9 2.7 tanh.8
  220.5 4.3 fusion.50
  224.9 2.6 reshape.142
  227.5 4.3 fusion.53
  231.8 2.0 reshape.139
  233.8 2.7 negate_add_fusion
  236.5 4.0 divide_multiply_fusion
  240.5 237.3 %while.12 = (s32[]{:T(128)}, f32[2,128,64]{1,2,0:T(8,128)S(1)}, f32[16,64,2,128]{3,1,0,2:T(8,128)S(1)}, f32[16,64,2,64]{3,2,1,0:T(2,128)}, bf16[16,64,2,64]{3,2,...) while((s32[]{:T(128)}, f32[2,128,64]{1,2,0:T(8,128)S(1)}, ...), condition=%wide.region_4.5_spmd, body=%wide.region_2.4_spmd.sunk | while | flops 32329792 | bytes 2025073 | solution.py:226
  240.5 0.9 fusion.188
  241.4 1.2 bitcast_multiply_fusion.9
  244.1 9.8 %custom-call.8 = f32[2,1,64,64]{2,3,1,0:T(8,128)S(1)} custom-call(f32[2,1,64,64]{3,2,1,0:T(8,128)S(1)} %fusion.192), custom_call_target="InvertDiagBlocksLowerTriangular" | custom-call | tf_op jit(solution)/shard_map/while/body/eval_jaxpr/jit(_solve_triangular)/vmap()/triangular_solve | solution.py:132
  255.3 0.9 fusion.188
  256.3 1.2 bitcast_multiply_fusion.9
  259.0 9.8 %custom-call.8 = f32[2,1,64,64]{2,3,1,0:T(8,128)S(1)} custom-call(f32[2,1,64,64]{3,2,1,0:T(8,128)S(1)} %fusion.192), custom_call_target="InvertDiagBlocksLowerTriangular" | custom-call | tf_op jit(solution)/shard_map/while/body/eval_jaxpr/jit(_solve_triangular)/vmap()/triangular_solve | solution.py:132
  270.2 0.9 fusion.188
  271.1 1.2 bitcast_multiply_fusion.9
  273.8 9.8 %custom-call.8 = f32[2,1,64,64]{2,3,1,0:T(8,128)S(1)} custom-call(f32[2,1,64,64]{3,2,1,0:T(8,128)S(1)} %fusion.192), custom_call_target="InvertDiagBlocksLowerTriangular" | custom-call | tf_op jit(solution)/shard_map/while/body/eval_jaxpr/jit(_solve_triangular)/vmap()/triangular_solve | solution.py:132
  285.0 0.9 fusion.188
  285.9 1.2 bitcast_multiply_fusion.9
  288.6 9.9 %custom-call.8 = f32[2,1,64,64]{2,3,1,0:T(8,128)S(1)} custom-call(f32[2,1,64,64]{3,2,1,0:T(8,128)S(1)} %fusion.192), custom_call_target="InvertDiagBlocksLowerTriangular" | custom-call | tf_op jit(solution)/shard_map/while/body/eval_jaxpr/jit(_solve_triangular)/vmap()/triangular_solve | solution.py:132
  299.8 0.9 fusion.188
  300.8 1.2 bitcast_multiply_fusion.9
  303.5 9.9 %custom-call.8 = f32[2,1,64,64]{2,3,1,0:T(8,128)S(1)} custom-call(f32[2,1,64,64]{3,2,1,0:T(8,128)S(1)} %fusion.192), custom_call_target="InvertDiagBlocksLowerTriangular" | custom-call | tf_op jit(solution)/shard_map/while/body/eval_jaxpr/jit(_solve_triangular)/vmap()/triangular_solve | solution.py:132
  314.7 0.9 fusion.188
  315.6 1.2 bitcast_multiply_fusion.9
  318.3 9.8 %custom-call.8 = f32[2,1,64,64]{2,3,1,0:T(8,128)S(1)} custom-call(f32[2,1,64,64]{3,2,1,0:T(8,128)S(1)} %fusion.192), custom_call_target="InvertDiagBlocksLowerTriangular" | custom-call | tf_op jit(solution)/shard_map/while/body/eval_jaxpr/jit(_solve_triangular)/vmap()/triangular_solve | solution.py:132
  330.4 1.2 bitcast_multiply_fusion.9
  333.1 9.8 %custom-call.8 = f32[2,1,64,64]{2,3,1,0:T(8,128)S(1)} custom-call(f32[2,1,64,64]{3,2,1,0:T(8,128)S(1)} %fusion.192), custom_call_target="InvertDiagBlocksLowerTriangular" | custom-call | tf_op jit(solution)/shard_map/while/body/eval_jaxpr/jit(_solve_triangular)/vmap()/triangular_solve | solution.py:132
  345.3 1.2 bitcast_multiply_fusion.9
  347.9 9.8 %custom-call.8 = f32[2,1,64,64]{2,3,1,0:T(8,128)S(1)} custom-call(f32[2,1,64,64]{3,2,1,0:T(8,128)S(1)} %fusion.192), custom_call_target="InvertDiagBlocksLowerTriangular" | custom-call | tf_op jit(solution)/shard_map/while/body/eval_jaxpr/jit(_solve_triangular)/vmap()/triangular_solve | solution.py:132
  360.1 1.2 bitcast_multiply_fusion.9
  362.8 9.8 %custom-call.8 = f32[2,1,64,64]{2,3,1,0:T(8,128)S(1)} custom-call(f32[2,1,64,64]{3,2,1,0:T(8,128)S(1)} %fusion.192), custom_call_target="InvertDiagBlocksLowerTriangular" | custom-call | tf_op jit(solution)/shard_map/while/body/eval_jaxpr/jit(_solve_triangular)/vmap()/triangular_solve | solution.py:132
  374.9 1.2 bitcast_multiply_fusion.9
  377.6 9.8 %custom-call.8 = f32[2,1,64,64]{2,3,1,0:T(8,128)S(1)} custom-call(f32[2,1,64,64]{3,2,1,0:T(8,128)S(1)} %fusion.192), custom_call_target="InvertDiagBlocksLowerTriangular" | custom-call | tf_op jit(solution)/shard_map/while/body/eval_jaxpr/jit(_solve_triangular)/vmap()/triangular_solve | solution.py:132
  389.7 1.2 bitcast_multiply_fusion.9
  392.4 9.8 %custom-call.8 = f32[2,1,64,64]{2,3,1,0:T(8,128)S(1)} custom-call(f32[2,1,64,64]{3,2,1,0:T(8,128)S(1)} %fusion.192), custom_call_target="InvertDiagBlocksLowerTriangular" | custom-call | tf_op jit(solution)/shard_map/while/body/eval_jaxpr/jit(_solve_triangular)/vmap()/triangular_solve | solution.py:132
  404.6 1.2 bitcast_multiply_fusion.9
  407.3 9.8 %custom-call.8 = f32[2,1,64,64]{2,3,1,0:T(8,128)S(1)} custom-call(f32[2,1,64,64]{3,2,1,0:T(8,128)S(1)} %fusion.192), custom_call_target="InvertDiagBlocksLowerTriangular" | custom-call | tf_op jit(solution)/shard_map/while/body/eval_jaxpr/jit(_solve_triangular)/vmap()/triangular_solve | solution.py:132
  419.4 1.2 bitcast_multiply_fusion.9
  422.1 9.8 %custom-call.8 = f32[2,1,64,64]{2,3,1,0:T(8,128)S(1)} custom-call(f32[2,1,64,64]{3,2,1,0:T(8,128)S(1)} %fusion.192), custom_call_target="InvertDiagBlocksLowerTriangular" | custom-call | tf_op jit(solution)/shard_map/while/body/eval_jaxpr/jit(_solve_triangular)/vmap()/triangular_solve | solution.py:132
  434.2 1.2 bitcast_multiply_fusion.9
  436.9 9.8 %custom-call.8 = f32[2,1,64,64]{2,3,1,0:T(8,128)S(1)} custom-call(f32[2,1,64,64]{3,2,1,0:T(8,128)S(1)} %fusion.192), custom_call_target="InvertDiagBlocksLowerTriangular" | custom-call | tf_op jit(solution)/shard_map/while/body/eval_jaxpr/jit(_solve_triangular)/vmap()/triangular_solve | solution.py:132
  449.1 1.2 bitcast_multiply_fusion.9
  451.7 9.8 %custom-call.8 = f32[2,1,64,64]{2,3,1,0:T(8,128)S(1)} custom-call(f32[2,1,64,64]{3,2,1,0:T(8,128)S(1)} %fusion.192), custom_call_target="InvertDiagBlocksLowerTriangular" | custom-call | tf_op jit(solution)/shard_map/while/body/eval_jaxpr/jit(_solve_triangular)/vmap()/triangular_solve | solution.py:132
  463.9 1.2 bitcast_multiply_fusion.9
  466.6 9.8 %custom-call.8 = f32[2,1,64,64]{2,3,1,0:T(8,128)S(1)} custom-call(f32[2,1,64,64]{3,2,1,0:T(8,128)S(1)} %fusion.192), custom_call_target="InvertDiagBlocksLowerTriangular" | custom-call | tf_op jit(solution)/shard_map/while/body/eval_jaxpr/jit(_solve_triangular)/vmap()/triangular_solve | solution.py:132
  479.0 7.5 %all-to-all-start = ((bf16[16,256,64]{1,2,0:T(8,128)(2,1)}), bf16[16,256,64]{1,2,0:T(8,128)(2,1)S(1)}, u32[]{:S(2)}, u32[]{:S(2)}) async-start(bf16[16,256,64]{1,2,0:T(8,128)(2,1)} %broadcast_in_dim.79), calls=%async_computation | async-start | bytes 1048576 | tf_op jit(solution)/shard_map/all_to_all | solution.py:27
  486.8 3.7 fusion.58
  490.5 2.3 fusion.57
  492.9 3.8 collective-permute-start
  498.0 10.0 %fusion.79 = f32[1024,2048]{1,0:T(8,128)} fusion(bf16[2048,256]{1,0:T(8,128)(2,1)} %all-gather.8.cloned.1.call-done, f32[2,128]{1,0:T(2,128)S(1)} %collective-permute-done, f32[1024,128]{1,0:T(8,128)S(1)} %fusion.57, bf16[1024,2048]{1,0:T(8,128)(2,1)} %all-gather.4.cloned.1.call-done, bf16[2048,1024]{1,0:T(8,128)(2,1)} %all-gather.6.cloned.1.call-done, ...), kind=kOutput, calls=%fused_computation.125 | convolution fusion | flops 1075183616 | bytes 14158336 | tf_op jit(solution)/shard_map/dot_general | solution.py:260
  511.1 6.8 %add_convert_fusion = bf16[1024,2048]{1,0:T(8,128)(2,1)} fusion(f32[1024,2048]{1,0:T(8,128)} %fusion.79, bf16[1024,128]{0,1:T(8,128)(2,1)S(1)} %bitcast.179, bf16[2048,256]{1,0:T(8,128)(2,1)} %all-gather.8.cloned.1.call-done), kind=kOutput, calls=%fused_computation.74 | convolution fusion | flops 541065216 | bytes 13369344 | tf_op jit(solution)/shard_map/dot_general | solution.py:261
  517.9 49.1 %reduce-scatter.2.cloned.1.call-done = bf16[128,2048]{1,0:T(8,128)(2,1)} async-done(((bf16[1024,2048]{1,0:T(8,128)(2,1)}), bf16[128,2048]{1,0:T(8,128)(2,1)}) %reduce-scatter.2.cloned.1.call-update) | async-done | bytes 524304 | tf_op jit(solution)/shard_map/reduce_scatter | solution.py:258
  (354 shorter events, 68.0 us)
Async XLA Ops:
  6.5 503.9 %copy-start = (f32[1,2,64,64]{3,2,1,0:T(8,128)S(1)}, f32[1,2,64,64]{3,2,1,0:T(8,128)}, u32[]{:S(2)}) copy-start(f32[1,2,64,64]{3,2,1,0:T(8,128)} %param.34) | copy-start | bytes 98308
  6.5 47.6 %all-gather.4.cloned.1.call-start = ((), (), s32[]{:S(2)}) async-start(), calls=%async_computation.2 | async-start | bytes 4718592 | tf_op jit(solution)/shard_map/all_gather | solution.py:192
  9.9 191.9 %all-gather.6.cloned.1.call-start = ((), (), s32[]{:S(2)}) async-start(), calls=%async_computation.3 | async-start | bytes 4259840 | tf_op jit(solution)/shard_map/all_gather | solution.py:21
  15.5 0.6 copy-start.2
  16.2 480.9 %all-gather.8.cloned.1.call-start = ((), (), s32[]{:S(2)}) async-start(), calls=%async_computation.4 | async-start | bytes 1064960 | tf_op jit(solution)/shard_map/all_gather | solution.py:76
  240.5 246.3 %copy-start.3 = (f32[3,128]{1,0:T(4,128)S(1)}, f32[3,128]{1,0:T(4,128)}, u32[]{:S(2)}) copy-start(f32[3,128]{1,0:T(4,128)} %param.25) | copy-start | bytes 4612
  479.0 29.0 %all-to-all-start = ((bf16[16,256,64]{1,2,0:T(8,128)(2,1)}), bf16[16,256,64]{1,2,0:T(8,128)(2,1)S(1)}, u32[]{:S(2)}, u32[]{:S(2)}) async-start(bf16[16,256,64]{1,2,0:T(8,128)(2,1)} %broadcast_in_dim.79), calls=%async_computation | async-start | bytes 1048576 | tf_op jit(solution)/shard_map/all_to_all | solution.py:27
  486.6 80.5 %reduce-scatter.2.cloned.1.call-start = ((), (), s32[]{:S(2)}) async-start(), calls=%async_computation.5 | async-start | bytes 4718592 | tf_op jit(solution)/shard_map/reduce_scatter | solution.py:258
  486.8 3.7 copy-start.1
  490.5 6.2 %copy-start.4 = (f32[128]{0:T(128)S(1)}, f32[128]{0:T(128)}, u32[]{:S(2)}) copy-start(f32[128]{0:T(128)} %param.35) | copy-start | bytes 1540
  492.9 5.1 collective-permute-start
Sparse Core Ops, SparseCore 0:
  10.0 44.0 all-gather.3
  57.0 144.6 all-gather.5
  204.7 136.9 all-gather.7
  518.1 48.9 reduce-scatter.1
where the time goes:
time: 577 us; the launch traced here: 574 us
  waiting for transfers between devices  230 us (40%)
  other arithmetic  205 us (36%)
  matrix products  75.6 us (13%)
  local copies, waits for them, and re-layouts  36.4 us (6%)
  between operations  13.5 us (2%)
  starting transfers between devices  11.7 us (2%)
    another operation x32, other arithmetic, block_pass(): jax.scipy.linalg.solve_triangular(system, right_side, lower=True, unit_di...  157 us
    all_gather x1, waiting for transfers between devices, side_by_side(): out = lax.all_gather(both, axis, axis=dim, tiled=True)  148 us
    reduce_scatter x1, waiting for transfers between devices, on_device(): lax.psum_scatter((jnp.dot(conv_mixed, conv_whole, preferred_element_type=...  49.1 us
    all_gather x1, waiting for transfers between devices, on_device(): piece = lax.all_gather(normed, 'tp', axis=0, tiled=True)  32.2 us
    dot_general x7, matrix products, project(): jnp.dot(activations, weight, preferred_element_type=jnp.float32)  27.1 us
    mul x16, other arithmetic, block_pass(): ask_reads = queries * jnp.exp(cumulative - middle)  19.7 us
    another operation x16, other arithmetic, block_pass(): cumulative = jnp.cumsum(logarithm_decay, axis=0)  14.6 us
    dynamic_slice x32, local copies, waits for them, and re-layouts, on_device(): lax.scan(block_pass, initial_rows, tuple((in_blocks(array) for array in (...  12.7 us
  transfers between devices with their start and end apart: 6, of which 4 were waited for; matrix products, arithmetic and copies ran while one was open for 53% of the time, Pallas kernels for 0%

commit v1 on v0

--- a/solution.py
+++ b/solution.py
@@ -189,7 +189,8 @@
         0,
         1,
     )
-    piece = lax.all_gather(normed, "tp", axis=0, tiled=True)
+    sent = jnp.stack([normed] * lax.axis_size("tp"))
+    piece = jnp.concatenate(lax.all_to_all(sent, "tp", 0, 0), axis=0)
     projected = jnp.concatenate([project(piece, weight) for weight in gathered], axis=1)
     pieces = jnp.split(projected, 8, axis=1)
     conv_mixed = conv_branch(pieces[0], pieces[1], pieces[2], convolution_taps)

time: 577 us -> 537 us (0.931)
  waiting for transfers between devices: 230 us -> 186 us
    all_gather x1, waiting for transfers between devices: 148 us -> 89.7 us  [side_by_side(): out = lax.all_gather(both, axis, axis=dim, tiled=True)]
    all_to_all x0 -> x1, waiting for transfers between devices: none -> 46.9 us  [on_device(): piece = jnp.concatenate(lax.all_to_all(sent, 'tp', 0, 0), axis=0)]
    all_gather x1 -> x0, waiting for transfers between devices: 32.2 us -> none  [on_device(): piece = lax.all_gather(normed, 'tp', axis=0, tiled=True)]
  transfers between devices with their start and end apart: 6 -> 6, of which waited for: 4 -> 4; matrix products, arithmetic and copies ran while one was open for 53% -> 56% of each run, Pallas kernels for 0% -> 0%
where the time goes in v1:
time: 537 us; the launch traced here: 534 us
  other arithmetic  204 us (38%)
  waiting for transfers between devices  186 us (35%)
  matrix products  76.8 us (14%)
  local copies, waits for them, and re-layouts  36.6 us (7%)
  starting transfers between devices  16.2 us (3%)
  between operations  13.5 us (3%)
    another operation x32, other arithmetic, block_pass(): jax.scipy.linalg.solve_triangular(system, right_side, lower=True, unit_di...  157 us
    all_gather x1, waiting for transfers between devices, side_by_side(): out = lax.all_gather(both, axis, axis=dim, tiled=True)  89.7 us
    reduce_scatter x1, waiting for transfers between devices, on_device(): lax.psum_scatter((jnp.dot(conv_mixed, conv_whole, preferred_element_type=...  48.2 us
    all_to_all x1, waiting for transfers between devices, on_device(): piece = jnp.concatenate(lax.all_to_all(sent, 'tp', 0, 0), axis=0)  46.9 us
    dot_general x7, matrix products, project(): jnp.dot(activations, weight, preferred_element_type=jnp.float32)  28.3 us
    mul x16, other arithmetic, block_pass(): ask_reads = queries * jnp.exp(cumulative - middle)  19.7 us
    another operation x16, other arithmetic, block_pass(): cumulative = jnp.cumsum(logarithm_decay, axis=0)  14.6 us
    dynamic_slice x32, local copies, waits for them, and re-layouts, on_device(): lax.scan(block_pass, initial_rows, tuple((in_blocks(array) for array in (...  12.7 us
  transfers between devices with their start and end apart: 6, of which 4 were waited for; matrix products, arithmetic and copies ran while one was open for 56% of the time, Pallas kernels for 0%

profile of v1, /device:TPU:8, one launch (start us, length us, event | category | flops | bytes accessed | tf_op | source)
XLA Modules:
  0.0 533.9 jit_solution(17773656821805206523)
XLA Ops:
  12.9 1.2 fusion.63
  14.1 1.2 fusion.73
  15.3 2.5 stack.5
  17.9 4.7 all-to-all-start
  23.5 1.6 reshape_squeeze.3
  25.3 46.9 %all-to-all-done = bf16[8,128,2048]{2,1,0:T(8,128)(2,1)} async-done(((bf16[8,128,2048]{2,1,0:T(8,128)(2,1)}), bf16[8,128,2048]{2,1,0:T(8,128)(2,1)}, u32[]{:S(2)}, u32[]{:S(2)}) %all-to-all-start) | async-done | bytes 4194336 | tf_op jit(solution)/shard_map/all_to_all | solution.py:193
  72.2 89.7 %all-gather.3.cloned.1.call-done = bf16[2048,1024]{1,0:T(8,128)(2,1)} async-done(((bf16[32,1024]{1,0:T(8,128)(2,1)}), bf16[2048,1024]{1,0:T(8,128)(2,1)}) %all-gather.3.cloned.1.call-update) | async-done | bytes 4194320 | tf_op jit(solution)/shard_map/all_gather | solution.py:21
  161.9 3.8 bitcast_reduce_fusion
  166.7 1.1 copy.76
  167.8 4.3 fusion.51
  172.1 1.6 reshape.158
  173.8 4.4 fusion.55
  178.1 2.6 tanh.8
  180.8 4.3 fusion.50
  185.1 2.6 reshape.159
  187.7 4.3 fusion.53
  192.0 2.0 reshape.156
  194.0 2.7 negate_add_fusion
  196.7 4.0 divide_multiply_fusion
  200.8 237.3 %while.12 = (s32[]{:T(128)}, f32[2,128,64]{1,2,0:T(8,128)S(1)}, f32[16,64,2,128]{3,1,0,2:T(8,128)S(1)}, f32[16,64,2,64]{3,2,1,0:T(2,128)}, bf16[16,64,2,64]{3,2,...) while((s32[]{:T(128)}, f32[2,128,64]{1,2,0:T(8,128)S(1)}, ...), condition=%wide.region_4.5_spmd, body=%wide.region_2.4_spmd.sunk | while | flops 32329792 | bytes 2025073 | solution.py:227
  200.8 0.9 fusion.189
  201.7 1.2 bitcast_multiply_fusion.9
  204.4 9.8 %custom-call.8 = f32[2,1,64,64]{2,3,1,0:T(8,128)S(1)} custom-call(f32[2,1,64,64]{3,2,1,0:T(8,128)S(1)} %fusion.193), custom_call_target="InvertDiagBlocksLowerTriangular" | custom-call | tf_op jit(solution)/shard_map/while/body/eval_jaxpr/jit(_solve_triangular)/vmap()/triangular_solve | solution.py:132
  215.6 0.9 fusion.189
  216.5 1.2 bitcast_multiply_fusion.9
  219.2 9.8 %custom-call.8 = f32[2,1,64,64]{2,3,1,0:T(8,128)S(1)} custom-call(f32[2,1,64,64]{3,2,1,0:T(8,128)S(1)} %fusion.193), custom_call_target="InvertDiagBlocksLowerTriangular" | custom-call | tf_op jit(solution)/shard_map/while/body/eval_jaxpr/jit(_solve_triangular)/vmap()/triangular_solve | solution.py:132
  230.4 0.9 fusion.189
  231.3 1.2 bitcast_multiply_fusion.9
  234.0 9.8 %custom-call.8 = f32[2,1,64,64]{2,3,1,0:T(8,128)S(1)} custom-call(f32[2,1,64,64]{3,2,1,0:T(8,128)S(1)} %fusion.193), custom_call_target="InvertDiagBlocksLowerTriangular" | custom-call | tf_op jit(solution)/shard_map/while/body/eval_jaxpr/jit(_solve_triangular)/vmap()/triangular_solve | solution.py:132
  245.2 0.9 fusion.189
  246.2 1.3 bitcast_multiply_fusion.9
  248.9 9.9 %custom-call.8 = f32[2,1,64,64]{2,3,1,0:T(8,128)S(1)} custom-call(f32[2,1,64,64]{3,2,1,0:T(8,128)S(1)} %fusion.193), custom_call_target="InvertDiagBlocksLowerTriangular" | custom-call | tf_op jit(solution)/shard_map/while/body/eval_jaxpr/jit(_solve_triangular)/vmap()/triangular_solve | solution.py:132
  260.1 0.9 fusion.189
  261.0 1.2 bitcast_multiply_fusion.9
  263.7 9.9 %custom-call.8 = f32[2,1,64,64]{2,3,1,0:T(8,128)S(1)} custom-call(f32[2,1,64,64]{3,2,1,0:T(8,128)S(1)} %fusion.193), custom_call_target="InvertDiagBlocksLowerTriangular" | custom-call | tf_op jit(solution)/shard_map/while/body/eval_jaxpr/jit(_solve_triangular)/vmap()/triangular_solve | solution.py:132
  275.8 1.2 bitcast_multiply_fusion.9
  278.5 9.8 %custom-call.8 = f32[2,1,64,64]{2,3,1,0:T(8,128)S(1)} custom-call(f32[2,1,64,64]{3,2,1,0:T(8,128)S(1)} %fusion.193), custom_call_target="InvertDiagBlocksLowerTriangular" | custom-call | tf_op jit(solution)/shard_map/while/body/eval_jaxpr/jit(_solve_triangular)/vmap()/triangular_solve | solution.py:132
  290.7 1.2 bitcast_multiply_fusion.9
  293.4 9.8 %custom-call.8 = f32[2,1,64,64]{2,3,1,0:T(8,128)S(1)} custom-call(f32[2,1,64,64]{3,2,1,0:T(8,128)S(1)} %fusion.193), custom_call_target="InvertDiagBlocksLowerTriangular" | custom-call | tf_op jit(solution)/shard_map/while/body/eval_jaxpr/jit(_solve_triangular)/vmap()/triangular_solve | solution.py:132
  305.5 1.2 bitcast_multiply_fusion.9
  308.2 9.8 %custom-call.8 = f32[2,1,64,64]{2,3,1,0:T(8,128)S(1)} custom-call(f32[2,1,64,64]{3,2,1,0:T(8,128)S(1)} %fusion.193), custom_call_target="InvertDiagBlocksLowerTriangular" | custom-call | tf_op jit(solution)/shard_map/while/body/eval_jaxpr/jit(_solve_triangular)/vmap()/triangular_solve | solution.py:132
  320.3 1.2 bitcast_multiply_fusion.9
  323.0 9.8 %custom-call.8 = f32[2,1,64,64]{2,3,1,0:T(8,128)S(1)} custom-call(f32[2,1,64,64]{3,2,1,0:T(8,128)S(1)} %fusion.193), custom_call_target="InvertDiagBlocksLowerTriangular" | custom-call | tf_op jit(solution)/shard_map/while/body/eval_jaxpr/jit(_solve_triangular)/vmap()/triangular_solve | solution.py:132
  335.2 1.2 bitcast_multiply_fusion.9
  337.9 9.8 %custom-call.8 = f32[2,1,64,64]{2,3,1,0:T(8,128)S(1)} custom-call(f32[2,1,64,64]{3,2,1,0:T(8,128)S(1)} %fusion.193), custom_call_target="InvertDiagBlocksLowerTriangular" | custom-call | tf_op jit(solution)/shard_map/while/body/eval_jaxpr/jit(_solve_triangular)/vmap()/triangular_solve | solution.py:132
  350.0 1.2 bitcast_multiply_fusion.9
  352.7 9.8 %custom-call.8 = f32[2,1,64,64]{2,3,1,0:T(8,128)S(1)} custom-call(f32[2,1,64,64]{3,2,1,0:T(8,128)S(1)} %fusion.193), custom_call_target="InvertDiagBlocksLowerTriangular" | custom-call | tf_op jit(solution)/shard_map/while/body/eval_jaxpr/jit(_solve_triangular)/vmap()/triangular_solve | solution.py:132
  364.8 1.2 bitcast_multiply_fusion.9
  367.5 9.8 %custom-call.8 = f32[2,1,64,64]{2,3,1,0:T(8,128)S(1)} custom-call(f32[2,1,64,64]{3,2,1,0:T(8,128)S(1)} %fusion.193), custom_call_target="InvertDiagBlocksLowerTriangular" | custom-call | tf_op jit(solution)/shard_map/while/body/eval_jaxpr/jit(_solve_triangular)/vmap()/triangular_solve | solution.py:132
  379.6 1.2 bitcast_multiply_fusion.9
  382.3 9.8 %custom-call.8 = f32[2,1,64,64]{2,3,1,0:T(8,128)S(1)} custom-call(f32[2,1,64,64]{3,2,1,0:T(8,128)S(1)} %fusion.193), custom_call_target="InvertDiagBlocksLowerTriangular" | custom-call | tf_op jit(solution)/shard_map/while/body/eval_jaxpr/jit(_solve_triangular)/vmap()/triangular_solve | solution.py:132
  394.5 1.2 bitcast_multiply_fusion.9
  397.2 9.8 %custom-call.8 = f32[2,1,64,64]{2,3,1,0:T(8,128)S(1)} custom-call(f32[2,1,64,64]{3,2,1,0:T(8,128)S(1)} %fusion.193), custom_call_target="InvertDiagBlocksLowerTriangular" | custom-call | tf_op jit(solution)/shard_map/while/body/eval_jaxpr/jit(_solve_triangular)/vmap()/triangular_solve | solution.py:132
  409.3 1.2 bitcast_multiply_fusion.9
  412.0 9.8 %custom-call.8 = f32[2,1,64,64]{2,3,1,0:T(8,128)S(1)} custom-call(f32[2,1,64,64]{3,2,1,0:T(8,128)S(1)} %fusion.193), custom_call_target="InvertDiagBlocksLowerTriangular" | custom-call | tf_op jit(solution)/shard_map/while/body/eval_jaxpr/jit(_solve_triangular)/vmap()/triangular_solve | solution.py:132
  424.1 1.2 bitcast_multiply_fusion.9
  426.8 9.8 %custom-call.8 = f32[2,1,64,64]{2,3,1,0:T(8,128)S(1)} custom-call(f32[2,1,64,64]{3,2,1,0:T(8,128)S(1)} %fusion.193), custom_call_target="InvertDiagBlocksLowerTriangular" | custom-call | tf_op jit(solution)/shard_map/while/body/eval_jaxpr/jit(_solve_triangular)/vmap()/triangular_solve | solution.py:132
  439.3 7.5 %all-to-all-start.1 = ((bf16[16,256,64]{1,2,0:T(8,128)(2,1)}), bf16[16,256,64]{1,2,0:T(8,128)(2,1)S(1)}, u32[]{:S(2)}, u32[]{:S(2)}) async-start(bf16[16,256,64]{1,2,0:T(8,128)(2,1)} %broadcast_in_dim.79), calls=%async_computation.1 | async-start | bytes 1048576 | tf_op jit(solution)/shard_map/all_to_all | solution.py:27
  446.9 3.5 fusion.58
  450.4 3.6 fusion.57
  454.0 3.8 collective-permute-start
  459.1 10.1 %fusion.80 = f32[1024,2048]{1,0:T(8,128)} fusion(bf16[2048,256]{1,0:T(8,128)(2,1)} %all-gather.5.cloned.1.call-done, f32[2,128]{1,0:T(2,128)S(1)} %collective-permute-done, f32[1024,128]{1,0:T(8,128)S(1)} %fusion.57, bf16[1024,2048]{1,0:T(8,128)(2,1)} %bitcast.15, bf16[2048,1024]{1,0:T(8,128)(2,1)} %all-gather.3.cloned.1.call-done, ...), kind=kOutput, calls=%fused_computation.126 | convolution fusion | flops 1075183616 | bytes 14158336 | tf_op jit(solution)/shard_map/dot_general | solution.py:261
  472.3 6.8 %add_convert_fusion = bf16[1024,2048]{1,0:T(8,128)(2,1)} fusion(f32[1024,2048]{1,0:T(8,128)} %fusion.80, bf16[1024,128]{0,1:T(8,128)(2,1)S(1)} %bitcast.178, bf16[2048,256]{1,0:T(8,128)(2,1)} %all-gather.5.cloned.1.call-done), kind=kOutput, calls=%fused_computation.74 | convolution fusion | flops 541065216 | bytes 13369344 | tf_op jit(solution)/shard_map/dot_general | solution.py:262
  479.1 48.2 %reduce-scatter.2.cloned.1.call-done = bf16[128,2048]{1,0:T(8,128)(2,1)} async-done(((bf16[1024,2048]{1,0:T(8,128)(2,1)}), bf16[128,2048]{1,0:T(8,128)(2,1)}) %reduce-scatter.2.cloned.1.call-update) | async-done | bytes 524304 | tf_op jit(solution)/shard_map/reduce_scatter | solution.py:259
  (362 shorter events, 68.1 us)
Async XLA Ops:
  6.5 465.1 %copy-start = (f32[1,2,64,64]{3,2,1,0:T(8,128)S(1)}, f32[1,2,64,64]{3,2,1,0:T(8,128)}, u32[]{:S(2)}) copy-start(f32[1,2,64,64]{3,2,1,0:T(8,128)} %param.34) | copy-start | bytes 98308
  6.5 155.4 %all-gather.3.cloned.1.call-start = ((), (), s32[]{:S(2)}) async-start(), calls=%async_computation.3 | async-start | bytes 4259840 | tf_op jit(solution)/shard_map/all_gather | solution.py:21
  12.2 0.6 copy-start.2
  17.8 4.8 copy-start.3
  17.8 4.8 copy-start.4
  17.8 5.5 %copy-start.6 = (f32[128]{0:T(128)S(1)}, f32[128]{0:T(128)}, u32[]{:S(2)}) copy-start(f32[128]{0:T(128)} %param.32) | copy-start | bytes 1540
  17.8 5.6 %copy-start.1 = (f32[1,1024,128]{2,1,0:T(8,128)S(1)}, f32[1,1024,128]{2,1,0:T(8,128)}, u32[]{:S(2)}) copy-start(f32[1,1024,128]{2,1,0:T(8,128)} %param.33) | copy-start | bytes 1572868
  17.8 7.2 %copy-start.7 = (f32[128]{0:T(128)S(1)}, f32[128]{0:T(128)}, u32[]{:S(2)}) copy-start(f32[128]{0:T(128)} %param.31) | copy-start | bytes 1540
  17.9 54.4 %all-to-all-start = ((bf16[8,128,2048]{2,1,0:T(8,128)(2,1)}), bf16[8,128,2048]{2,1,0:T(8,128)(2,1)}, u32[]{:S(2)}, u32[]{:S(2)}) async-start(bf16[8,128,2048]{2,1,0:T(8,128)(2,1)} %stack.5), calls=%async_computation | async-start | bytes 8388608 | tf_op jit(solution)/shard_map/all_to_all | solution.py:193
  22.6 435.7 %all-gather.5.cloned.1.call-start = ((), (), s32[]{:S(2)}) async-start(), calls=%async_computation.4 | async-start | bytes 1064960 | tf_op jit(solution)/shard_map/all_gather | solution.py:76
  200.7 246.1 %copy-start.5 = (f32[3,128]{1,0:T(4,128)S(1)}, f32[3,128]{1,0:T(4,128)}, u32[]{:S(2)}) copy-start(f32[3,128]{1,0:T(4,128)} %param.25) | copy-start | bytes 4612
  439.3 29.9 %all-to-all-start.1 = ((bf16[16,256,64]{1,2,0:T(8,128)(2,1)}), bf16[16,256,64]{1,2,0:T(8,128)(2,1)S(1)}, u32[]{:S(2)}, u32[]{:S(2)}) async-start(bf16[16,256,64]{1,2,0:T(8,128)(2,1)} %broadcast_in_dim.79), calls=%async_computation.1 | async-start | bytes 1048576 | tf_op jit(solution)/shard_map/all_to_all | solution.py:27
  446.8 80.5 %reduce-scatter.2.cloned.1.call-start = ((), (), s32[]{:S(2)}) async-start(), calls=%async_computation.5 | async-start | bytes 4718592 | tf_op jit(solution)/shard_map/reduce_scatter | solution.py:259
  450.4 7.4 %copy-start.8 = (f32[128]{0:T(128)S(1)}, f32[128]{0:T(128)}, u32[]{:S(2)}) copy-start(f32[128]{0:T(128)} %param.35) | copy-start | bytes 1540
  454.0 5.1 collective-permute-start
Sparse Core Ops, SparseCore 0:
  13.0 148.9 all-gather.2
  164.9 137.2 all-gather.4
  479.2 48.0 reduce-scatter.1
